TPU v7x, 128 devices: a whole 4x4x4 slice. The times are simulated.
128 devices in a mesh: fs: 16 (over z, x), tp: 8 (over y, core).
Axes of the slice: x: 4, y: 4, z: 4, core: 2. Of those that a mesh axis runs over, the one named last changes fastest.
Arguments:
- later_input: bfloat16 [12288, 2048], P('fs', 'tp'), may hold values from -6 to 6
- earlier_input: bfloat16 [12288, 2048], P('fs', 'tp'), may hold values from -6 to 6
- cotangent: bfloat16 [12288, 2048], P('fs', 'tp'), may hold values from -6 to 6
- up_weight: bfloat16 [2048, 8192], P('fs', 'tp'), may hold values from -0.125 to 0.125
- down_weight: bfloat16 [8192, 2048], P('tp', 'fs'), may hold values from -0.0625 to 0.0625
- up_running: float32 [2048, 8192], P('fs', 'tp'), may hold values from -6 to 6
- down_running: float32 [2048, 8192], P('fs', 'tp'), may hold values from -6 to 6
Outputs:
- later_output: bfloat16 [12288, 2048], P('fs', 'tp')
- later_preact: bfloat16 [12288, 8192], P('fs', 'tp')
- earlier_grad: bfloat16 [12288, 2048], P('fs', 'tp')
- up_running_out: float32 [2048, 8192], P('fs', 'tp')
- down_running_out: float32 [2048, 8192], P('fs', 'tp')
All inputs are finite; a program needn't handle non-finite values.
Results may differ from a plain program's by a relative error of at most 0.014.
Values may be sent and summed in bfloat16 or wider, within the bound.
A program may use at most 128 MiB of HBM per device.

v0:
```python
import jax
import jax.numpy as jnp
from jax import lax
from jax.sharding import PartitionSpec as P

contract_last = (((1,), (1,)), ((), ()))
contract_first = (((0,), (0,)), ((), ()))


def in_one_piece(arrays, axis, dim, along):
    ends, at = ([], 0)
    for a in arrays[:-1]:
        at += a.shape[along]
        ends.append(at)
    both = jnp.concatenate(arrays, axis=along)
    return tuple(jnp.split(lax.all_gather(both, axis, axis=dim, tiled=True), ends, axis=along))


def gather_turned(arrays, axis, dims):
    turned = [jnp.moveaxis(a, dim, 0) for a, dim in zip(arrays, dims)]
    widths = [t[0].size for t in turned]
    both = jnp.concatenate([t.reshape(-1, w) for t, w in zip(turned, widths)], axis=1)
    filled = lax.all_gather(both, axis, axis=0, tiled=True)
    tiles = jnp.split(filled, [sum(widths[:k]) for k in range(1, len(widths))], axis=1)
    return tuple(
        (
            jnp.moveaxis(b.reshape(-1, *t.shape[1:]), 0, dim)
            for b, t, dim in zip(tiles, turned, dims)
        )
    )


def side_by_side(arrays, axis, dim, along):
    both = jnp.concatenate(arrays, axis=along)
    filled, at, outs = (lax.psum_scatter(both, axis, scatter_dimension=dim, tiled=True), 0, [])
    for a in arrays:
        outs.append(lax.slice_in_dim(filled, at, at + a.shape[along], axis=along))
        at += a.shape[along]
    return tuple(outs)


def on_device(
    later_input, earlier_input, cotangent, up_weight, down_weight, up_running, down_running
):
    rows = later_input.shape[0]
    factor = float(rows * lax.axis_size("fs")) ** (-0.5)
    later_full, earlier_full, cot_full = in_one_piece(
        (later_input, earlier_input, cotangent), "tp", 1, 0
    )
    columns = up_weight.shape[1]
    up_whole, down_whole = gather_turned((up_weight, down_weight), "fs", (0, 1))
    later_up = jnp.dot(later_full, up_whole, preferred_element_type=jnp.float32)
    earlier_up = jnp.dot(earlier_full, up_whole, preferred_element_type=jnp.float32)
    later_hidden = jnp.square(jax.nn.relu(later_up)).astype(jnp.bfloat16)
    out_part = jnp.dot(later_hidden, down_whole, preferred_element_type=jnp.float32)
    hidden_grad = lax.dot_general(
        cot_full, down_whole, contract_last, preferred_element_type=jnp.float32
    )
    up_grad = (2.0 * jax.nn.relu(earlier_up) * hidden_grad).astype(jnp.bfloat16)
    back_part = lax.dot_general(
        up_grad, up_whole, contract_last, preferred_element_type=jnp.float32
    )
    later_preact = later_up.astype(jnp.bfloat16)
    earlier_hidden = jnp.square(jax.nn.relu(earlier_up)).astype(jnp.bfloat16)
    out_sum, back_sum = tuple(
        (
            part.astype(jnp.float32)
            for part in side_by_side(
                (out_part.astype(jnp.bfloat16), back_part.astype(jnp.bfloat16)), "tp", 1, 0
            )
        )
    )
    summed = lax.psum_scatter(
        jnp.concatenate(
            (
                lax.dot_general(
                    earlier_full, up_grad, contract_first, preferred_element_type=jnp.float32
                ),
                lax.dot_general(
                    cot_full, earlier_hidden, contract_first, preferred_element_type=jnp.float32
                ),
            ),
            axis=1,
        ).astype(jnp.bfloat16),
        "fs",
        scatter_dimension=0,
        tiled=True,
    ).astype(jnp.float32)
    grad_up_sum = summed[:, :columns]
    grad_down_sum = summed[:, columns:]
    return (
        out_sum.astype(jnp.bfloat16),
        later_preact,
        back_sum.astype(jnp.bfloat16),
        up_running + grad_up_sum * factor,
        down_running + grad_down_sum * factor,
    )


def solution(mesh):
    in_specs = (
        P("fs", "tp"),
        P("fs", "tp"),
        P("fs", "tp"),
        P("fs", "tp"),
        P("tp", "fs"),
        P("fs", "tp"),
        P("fs", "tp"),
    )
    out_specs = (P("fs", "tp"), P("fs", "tp"), P("fs", "tp"), P("fs", "tp"), P("fs", "tp"))
    return jax.shard_map(
        on_device, mesh=mesh, in_specs=in_specs, out_specs=out_specs, check_vma=False
    )
```

profile of v0, /device:TPU:0, one launch (start us, length us, event | category | flops | bytes accessed | tf_op | source)
XLA Modules:
  0.0 322.6 jit_solution(7393562719880853422)
XLA Ops:
  7.2 0.0 all-gather.5.cloned.1.call-start
  7.2 1.1 copy.17
  8.3 1.8 pad_maximum_fusion.3
  10.1 0.0 all-gather.5.cloned.1.call-update
  10.1 0.0 all-gather.3.cloned.1.call-start
  10.2 2.3 pad_maximum_fusion.2
  12.5 0.0 reduce-scatter.5.cloned.1.call-start
  12.6 77.9 %all-gather.5.cloned.1.call-done = bf16[2048,2048]{0,1:T(8,128)(2,1)} async-done(((bf16[128,2048]{0,1:T(8,128)(2,1)}), bf16[2048,2048]{0,1:T(8,128)(2,1)}) %all-gather.5.cloned.1.call-update) | async-done | bytes 8388624 | tf_op jit(solution)/shard_map/all_gather | solution.py:23
  90.5 59.5 %all-gather.3.cloned.1.call-done = bf16[2304,2048]{1,0:T(8,128)(2,1)} async-done(((bf16[2304,256]{1,0:T(8,128)(2,1)}), bf16[2304,2048]{1,0:T(8,128)(2,1)}) %all-gather.3.cloned.1.call-update) | async-done | bytes 9437200 | tf_op jit(solution)/shard_map/all_gather | solution.py:16
  150.0 6.3 %fusion.8 = f32[768,1024]{1,0:T(8,128)S(1)} fusion(bf16[2048,2048]{0,1:T(8,128)(2,1)} %all-gather.5.cloned.1.call-done, bf16[2304,2048]{1,0:T(8,128)(2,1)} %all-gather.3.cloned.1.call-done), kind=kOutput, calls=%fused_computation.11 | convolution fusion | flops 3221225472 | bytes 10485760 | tf_op jit(solution)/shard_map/dot_general | solution.py:53
  156.4 1.9 copy-done.3
  158.3 4.7 %fusion.28 = (bf16[768,1024]{1,0:T(8,128)(2,1)}, f32[768,1024]{1,0:T(8,128)S(1)}) fusion(bf16[2048,2048]{0,1:T(8,128)(2,1)S(1)} %copy-done.3, bf16[2304,2048]{1,0:T(8,128)(2,1)S(1)} %copy-done.2), kind=kOutput, calls=%fused_computation.34 | convolution fusion | flops 3222011904 | bytes 12058624 | tf_op jit(solution)/shard_map/dot_general | solution.py:52
  163.0 3.6 %multiply_convert_fusion.1 = bf16[768,1024]{1,0:T(8,128)(2,1)S(1)} fusion(f32[768,1024]{1,0:T(8,128)S(1)} %fusion.8, bf16[2048,2048]{0,1:T(8,128)(2,1)S(1)} %copy-done.3, bf16[2304,2048]{1,0:T(8,128)(2,1)S(1)} %copy-done.2), kind=kOutput, calls=%fused_computation.17 | convolution fusion | flops 3224371200 | bytes 12058624 | tf_op jit(solution)/shard_map/dot_general | solution.py:56
  166.6 3.7 %convolution_convert_fusion.2 = bf16[768,2048]{1,0:T(8,128)(2,1)S(1)} fusion(bf16[768,1024]{1,0:T(8,128)(2,1)S(1)} %multiply_convert_fusion.1, bf16[2048,2048]{0,1:T(8,128)(2,1)S(1)} %copy-done.3), kind=kOutput, calls=%fused_computation.9 | convolution fusion | flops 3222798336 | bytes 8912896 | tf_op jit(solution)/shard_map/dot_general | solution.py:60
  170.2 5.9 %fusion.4 = bf16[768,2048]{1,0:T(8,128)(2,1)S(1)} fusion(bf16[2048,2048]{0,1:T(8,128)(2,1)} %all-gather.5.cloned.1.call-done, f32[768,1024]{1,0:T(8,128)S(1)} %get-tuple-element.20), kind=kOutput, calls=%fused_computation.8 | convolution fusion | flops 3225157632 | bytes 10485760 | tf_op jit(solution)/shard_map/dot_general | solution.py:55
  176.1 3.8 %pad_maximum_fusion.1 = bf16[1536,2048]{1,0:T(8,128)(2,1)} fusion(bf16[768,2048]{1,0:T(8,128)(2,1)S(1)} %convolution_convert_fusion.2, bf16[768,2048]{1,0:T(8,128)(2,1)S(1)} %fusion.4), kind=kLoop, calls=%fused_computation.1 | loop fusion | flops 12582912 | bytes 12582912 | tf_op jit(solution)/shard_map/concatenate | solution.py:34
  179.9 0.2 reduce-scatter.7.cloned.1.call-start
  180.2 8.0 %convolution_convert_fusion.1 = bf16[2048,1024]{0,1:T(8,128)(2,1)} fusion(bf16[768,1024]{1,0:T(8,128)(2,1)} %copy-done.6, bf16[2304,2048]{1,0:T(8,128)(2,1)} %all-gather.3.cloned.1.call-done), kind=kOutput, calls=%fused_computation.3 | convolution fusion | flops 3223322624 | bytes 8912896 | tf_op jit(solution)/shard_map/dot_general | solution.py:76
  188.2 7.3 %convolution_convert_fusion = bf16[2048,1024]{0,1:T(8,128)(2,1)} fusion(bf16[2304,2048]{1,0:T(8,128)(2,1)} %all-gather.3.cloned.1.call-done, f32[768,1024]{1,0:T(8,128)S(1)} %copy-done.5), kind=kOutput, calls=%fused_computation.2 | convolution fusion | flops 3225681920 | bytes 10485760 | tf_op jit(solution)/shard_map/dot_general | solution.py:79
  195.4 8.5 %pad_maximum_fusion = bf16[2048,2048]{0,1:T(8,128)(2,1)} fusion(bf16[2048,1024]{0,1:T(8,128)(2,1)} %convolution_convert_fusion, bf16[2048,1024]{0,1:T(8,128)(2,1)} %convolution_convert_fusion.1), kind=kLoop, calls=%fused_computation | loop fusion | flops 16777216 | bytes 16777216 | tf_op jit(solution)/shard_map/concatenate | solution.py:74
  204.0 12.3 %copy.22 = bf16[2048,2048]{1,0:T(8,128)(2,1)} copy(bf16[2048,2048]{0,1:T(8,128)(2,1)} %pad_maximum_fusion) | data formatting | bytes 16777216
  216.3 1.0 copy-done
  217.3 0.2 copy.19
  217.5 0.2 copy.18
  217.7 5.9 %reduce-scatter.5.cloned.1.call-done = bf16[1536,256]{1,0:T(8,128)(2,1)} async-done(((bf16[1536,2048]{1,0:T(8,128)(2,1)}), bf16[1536,256]{1,0:T(8,128)(2,1)}) %reduce-scatter.5.cloned.1.call-update) | async-done | bytes 786448 | tf_op jit(solution)/shard_map/reduce_scatter | solution.py:35
  223.6 2.0 fusion.27
  225.6 87.0 %reduce-scatter.7.cloned.1.call-done = bf16[128,2048]{1,0:T(8,128)(2,1)} async-done(((bf16[2048,2048]{1,0:T(8,128)(2,1)}), bf16[128,2048]{1,0:T(8,128)(2,1)}) %reduce-scatter.7.cloned.1.call-update) | async-done | bytes 524304
  312.6 1.3 copy.23
  313.9 0.1 convert_element_type.32
  314.0 0.1 fusion.23
  314.1 1.0 copy.20
  315.1 1.0 copy.21
  (15 shorter events, 0.1 us)
Async XLA Ops:
  7.2 83.4 %all-gather.5.cloned.1.call-start = ((), (), s32[]{:S(2)}) async-start(), calls=%async_computation.3 | async-start | bytes 8912896 | tf_op jit(solution)/shard_map/all_gather | solution.py:23
  10.1 139.9 %all-gather.3.cloned.1.call-start = ((), (), s32[]{:S(2)}) async-start(), calls=%async_computation.2 | async-start | bytes 10616832 | tf_op jit(solution)/shard_map/all_gather | solution.py:16
  12.5 211.0 %reduce-scatter.5.cloned.1.call-start = ((), (), s32[]{:S(2)}) async-start(), calls=%async_computation.4 | async-start | bytes 7077888 | tf_op jit(solution)/shard_map/reduce_scatter | solution.py:35
  150.0 6.4 %copy-start.2 = (bf16[2304,2048]{1,0:T(8,128)(2,1)S(1)}, bf16[2304,2048]{1,0:T(8,128)(2,1)}, u32[]{:S(2)}) copy-start(bf16[2304,2048]{1,0:T(8,128)(2,1)} %all-gather.3.cloned.1.call-done) | copy-start | bytes 28311556
  150.0 8.2 %copy-start.3 = (bf16[2048,2048]{0,1:T(8,128)(2,1)S(1)}, bf16[2048,2048]{0,1:T(8,128)(2,1)}, u32[]{:S(2)}) copy-start(bf16[2048,2048]{0,1:T(8,128)(2,1)} %all-gather.5.cloned.1.call-done) | copy-start | bytes 25165828
  158.3 4.7 %copy-start.4 = (f32[768,1024]{1,0:T(8,128)}, f32[768,1024]{1,0:T(8,128)S(1)}, u32[]{:S(2)}) copy-start(f32[768,1024]{1,0:T(8,128)S(1)} %fusion.8) | copy-start | bytes 9437188
  166.5 3.7 %copy-start.6 = (bf16[768,1024]{1,0:T(8,128)(2,1)}, bf16[768,1024]{1,0:T(8,128)(2,1)S(1)}, u32[]{:S(2)}) copy-start(bf16[768,1024]{1,0:T(8,128)(2,1)S(1)} %multiply_convert_fusion.1) | copy-start | bytes 4718596
  179.9 8.2 %copy-start.5 = (f32[768,1024]{1,0:T(8,128)S(1)}, f32[768,1024]{1,0:T(8,128)}, u32[]{:S(2)}) copy-start(f32[768,1024]{1,0:T(8,128)} %copy-done.4) | copy-start | bytes 9437188
  179.9 132.7 %reduce-scatter.7.cloned.1.call-start = ((), (), s32[]{:S(2)}) async-start(), calls=%async_computation.5 | async-start | bytes 8912896
  216.2 1.0 copy-start
  216.2 1.2 copy-start.1
Sparse Core Ops, SparseCore 0:
  10.7 79.8 all-gather.4
  92.8 57.2 all-gather.2
  180.0 43.4 reduce-scatter.4
  226.8 85.7 reduce-scatter.6
where the time goes:
time: 323 us
  waiting for transfers between devices  230 us (71%)
  matrix products  39.4 us (12%)
  local copies, waits for them, and re-layouts  22 us (7%)
  other arithmetic  16.6 us (5%)
  between operations  13.9 us (4%)
    unnamed x5, waiting for transfers between devices  87.1 us
    all_gather x1, waiting for transfers between devices, gather_turned(): filled = lax.all_gather(both, axis, axis=0, tiled=True)  77.9 us
    all_gather x1, waiting for transfers between devices, in_one_piece(): lax.all_gather(both, axis, axis=dim, tiled=True)  59.5 us
    unnamed x21, local copies, waits for them, and re-layouts  20 us
    concatenate x1, other arithmetic, on_device(): jnp.concatenate((lax.dot_general(earlier_full, up_grad, contract_first, p...  8.54 us
    dot_general x1, matrix products, on_device(): lax.dot_general(earlier_full, up_grad, contract_first, preferred_element_...  8 us
    dot_general x1, matrix products, on_device(): lax.dot_general(cot_full, earlier_hidden, contract_first, preferred_eleme...  7.27 us
  transfers between devices with their start and end apart: 4, of which 4 were waited for; matrix products, arithmetic and copies ran while one was open for 13% of the time, Pallas kernels for 0%

commit v1 on v0

--- a/solution.py
+++ b/solution.py
@@ -20,7 +20,9 @@
     turned = [jnp.moveaxis(a, dim, 0) for a, dim in zip(arrays, dims)]
     widths = [t[0].size for t in turned]
     both = jnp.concatenate([t.reshape(-1, w) for t, w in zip(turned, widths)], axis=1)
-    filled = lax.all_gather(both, axis, axis=0, tiled=True)
+    filled = jnp.concatenate(
+        lax.all_to_all(jnp.stack([both] * lax.axis_size(axis)), axis, 0, 0), axis=0
+    )
     tiles = jnp.split(filled, [sum(widths[:k]) for k in range(1, len(widths))], axis=1)
     return tuple(
         (

time: 323 us -> 285 us (0.88)
  waiting for transfers between devices: 230 us -> 89.8 us
  blocking collectives: 0 us -> 104 us
    all_to_all x0 -> x1, blocking collectives: none -> 104 us  [gather_turned(): lax.all_to_all(jnp.stack([both] * lax.axis_size(axis)), axis, 0, 0)]
    all_gather x1 -> x0, waiting for transfers between devices: 77.9 us -> none  [gather_turned(): filled = lax.all_gather(both, axis, axis=0, tiled=True)]
    all_gather x1, waiting for transfers between devices: 59.5 us -> 0.01 us  [in_one_piece(): lax.all_gather(both, axis, axis=dim, tiled=True)]
    unnamed x21 -> x25, local copies, waits for them, and re-layouts: 20 us -> 21.5 us
    unnamed x5 -> x4, waiting for transfers between devices: 87.1 us -> 87.1 us
  transfers between devices with their start and end apart: 4 -> 3, of which waited for: 4 -> 2; matrix products, arithmetic and copies ran while one was open for 13% -> 14% of each run, Pallas kernels for 0% -> 0%
where the time goes in v1:
time: 285 us; the launch traced here: 284 us
  blocking collectives  104 us (36%)
  waiting for transfers between devices  89.8 us (32%)
  matrix products  36.7 us (13%)
  local copies, waits for them, and re-layouts  24.8 us (9%)
  other arithmetic  14.9 us (5%)
  between operations  13.9 us (5%)
    all_to_all x1, blocking collectives, gather_turned(): lax.all_to_all(jnp.stack([both] * lax.axis_size(axis)), axis, 0, 0)  104 us
    unnamed x4, waiting for transfers between devices  87.1 us
    unnamed x25, local copies, waits for them, and re-layouts  21.5 us
    concatenate x1, other arithmetic, on_device(): jnp.concatenate((lax.dot_general(earlier_full, up_grad, contract_first, p...  8.55 us
    dot_general x1, matrix products, on_device(): lax.dot_general(earlier_full, up_grad, contract_first, preferred_element_...  8 us
    dot_general x1, matrix products, on_device(): lax.dot_general(cot_full, earlier_hidden, contract_first, preferred_eleme...  6.95 us
    dot_general x1, matrix products, on_device(): jnp.dot(earlier_full, up_whole, preferred_element_type=jnp.float32)  6.3 us
  transfers between devices with their start and end apart: 3, of which 2 were waited for; matrix products, arithmetic and copies ran while one was open for 14% of the time, Pallas kernels for 0%

profile of v1, /device:TPU:0, one launch (start us, length us, event | category | flops | bytes accessed | tf_op | source)
XLA Modules:
  0.0 284.2 jit_solution(4400937559740373198)
XLA Ops:
  7.2 0.0 all-gather.2.cloned.1.call-start
  7.2 2.4 pad_maximum_fusion.2
  9.6 0.0 reduce-scatter.5.cloned.1.call-start
  9.7 0.2 copy.18
  9.9 0.2 copy.19
  10.1 1.1 stack.2
  11.2 103.7 %all_to_all.5 = bf16[16,128,2048]{2,1,0:T(8,128)(2,1)} all-to-all(bf16[16,128,2048]{2,1,0:T(8,128)(2,1)S(1)} %stack.2), channel_id=1, replica_groups=mesh['fs'=16,'tp'=8] {'fs'}, dimensions={0} | all-to-all | bytes 16777216 | tf_op jit(solution)/shard_map/all_to_all | solution.py:24
  114.9 6.3 %fusion.8 = f32[768,1024]{1,0:T(8,128)S(1)} fusion(bf16[2048,2048]{1,0:T(8,128)(2,1)} %bitcast.5, bf16[2304,2048]{1,0:T(8,128)(2,1)} %all-gather.2.cloned.1.call-done), kind=kOutput, calls=%fused_computation.11 | convolution fusion | flops 3221225472 | bytes 10485760 | tf_op jit(solution)/shard_map/dot_general | solution.py:55
  121.2 1.8 copy-done.6
  123.0 1.3 copy-done.5
  124.3 3.5 %multiply_convert_fusion.1 = bf16[768,1024]{1,0:T(8,128)(2,1)S(1)} fusion(f32[768,1024]{1,0:T(8,128)S(1)} %fusion.8, bf16[2048,2048]{1,0:T(8,128)(2,1)S(1)} %bitcast.6, bf16[2304,2048]{1,0:T(8,128)(2,1)S(1)} %copy-done.5), kind=kOutput, calls=%fused_computation.17 | convolution fusion | flops 3224371200 | bytes 12058624 | tf_op jit(solution)/shard_map/dot_general | solution.py:58
  127.8 1.1 copy-done.8
  128.9 3.7 %convolution_convert_fusion.2 = bf16[768,2048]{1,0:T(8,128)(2,1)S(1)} fusion(bf16[768,1024]{1,0:T(8,128)(2,1)S(1)} %multiply_convert_fusion.1, bf16[2048,2048]{1,0:T(8,128)(2,1)S(1)} %bitcast.7), kind=kOutput, calls=%fused_computation.9 | convolution fusion | flops 3222798336 | bytes 8912896 | tf_op jit(solution)/shard_map/dot_general | solution.py:62
  132.6 4.6 %fusion.28 = (bf16[768,1024]{1,0:T(8,128)(2,1)}, f32[768,1024]{1,0:T(8,128)S(1)}) fusion(bf16[2048,2048]{1,0:T(8,128)(2,1)S(1)} %bitcast.8, bf16[2304,2048]{1,0:T(8,128)(2,1)S(1)} %copy-done.5), kind=kOutput, calls=%fused_computation.34 | convolution fusion | flops 3222011904 | bytes 12058624 | tf_op jit(solution)/shard_map/dot_general | solution.py:54
  137.2 3.7 %fusion.4 = bf16[768,2048]{1,0:T(8,128)(2,1)S(1)} fusion(bf16[2048,2048]{1,0:T(8,128)(2,1)S(1)} %bitcast.9, f32[768,1024]{1,0:T(8,128)S(1)} %get-tuple-element.20), kind=kOutput, calls=%fused_computation.8 | convolution fusion | flops 3225157632 | bytes 10485760 | tf_op jit(solution)/shard_map/dot_general | solution.py:57
  140.9 3.8 %pad_maximum_fusion.1 = bf16[1536,2048]{1,0:T(8,128)(2,1)} fusion(bf16[768,2048]{1,0:T(8,128)(2,1)S(1)} %convolution_convert_fusion.2, bf16[768,2048]{1,0:T(8,128)(2,1)S(1)} %fusion.4), kind=kLoop, calls=%fused_computation.1 | loop fusion | flops 12582912 | bytes 12582912 | tf_op jit(solution)/shard_map/concatenate | solution.py:36
  144.8 0.2 reduce-scatter.7.cloned.1.call-start
  145.0 8.0 %convolution_convert_fusion.1 = bf16[2048,1024]{0,1:T(8,128)(2,1)} fusion(bf16[768,1024]{1,0:T(8,128)(2,1)} %copy-done.8, bf16[2304,2048]{1,0:T(8,128)(2,1)} %all-gather.2.cloned.1.call-done), kind=kOutput, calls=%fused_computation.3 | convolution fusion | flops 3223322624 | bytes 8912896 | tf_op jit(solution)/shard_map/dot_general | solution.py:78
  153.0 7.0 %convolution_convert_fusion = bf16[2048,1024]{0,1:T(8,128)(2,1)} fusion(bf16[2304,2048]{1,0:T(8,128)(2,1)} %all-gather.2.cloned.1.call-done, f32[768,1024]{1,0:T(8,128)S(1)} %copy-done.7), kind=kOutput, calls=%fused_computation.2 | convolution fusion | flops 3225681920 | bytes 10485760 | tf_op jit(solution)/shard_map/dot_general | solution.py:81
  160.0 8.6 %pad_maximum_fusion = bf16[2048,2048]{0,1:T(8,128)(2,1)} fusion(bf16[2048,1024]{0,1:T(8,128)(2,1)} %convolution_convert_fusion, bf16[2048,1024]{0,1:T(8,128)(2,1)} %convolution_convert_fusion.1), kind=kLoop, calls=%fused_computation | loop fusion | flops 16777216 | bytes 16777216 | tf_op jit(solution)/shard_map/concatenate | solution.py:76
  168.5 12.4 %copy.24 = bf16[2048,2048]{1,0:T(8,128)(2,1)} copy(bf16[2048,2048]{0,1:T(8,128)(2,1)} %pad_maximum_fusion) | data formatting | bytes 16777216
  181.0 1.0 copy-done.1
  182.0 0.2 copy.21
  182.2 0.2 copy.20
  182.4 2.7 reduce-scatter.5.cloned.1.call-done
  185.1 2.0 fusion.27
  187.1 87.1 %reduce-scatter.7.cloned.1.call-done = bf16[128,2048]{1,0:T(8,128)(2,1)} async-done(((bf16[2048,2048]{1,0:T(8,128)(2,1)}), bf16[128,2048]{1,0:T(8,128)(2,1)}) %reduce-scatter.7.cloned.1.call-update) | async-done | bytes 524304
  274.2 1.3 copy.25
  275.5 0.1 convert_element_type.32
  275.6 0.1 fusion.23
  275.7 1.0 copy.22
  276.7 1.0 copy.23
  (19 shorter events, 0.1 us)
Async XLA Ops:
  7.2 2.5 copy-start.3
  7.2 2.7 copy-start.4
  7.2 107.7 %all-gather.2.cloned.1.call-start = ((), (), s32[]{:S(2)}) async-start(), calls=%async_computation.3 | async-start | bytes 10616832 | tf_op jit(solution)/shard_map/all_gather | solution.py:16
  9.6 175.4 %reduce-scatter.5.cloned.1.call-start = ((), (), s32[]{:S(2)}) async-start(), calls=%async_computation.4 | async-start | bytes 7077888 | tf_op jit(solution)/shard_map/reduce_scatter | solution.py:37
  114.9 8.1 %copy-start = (bf16[16,128,2048]{2,1,0:T(8,128)(2,1)S(1)}, bf16[16,128,2048]{2,1,0:T(8,128)(2,1)}, u32[]{:S(2)}) copy-start(bf16[16,128,2048]{2,1,0:T(8,128)(2,1)} %all_to_all.5) | copy-start | bytes 25165828
  114.9 9.4 %copy-start.5 = (bf16[2304,2048]{1,0:T(8,128)(2,1)S(1)}, bf16[2304,2048]{1,0:T(8,128)(2,1)}, u32[]{:S(2)}) copy-start(bf16[2304,2048]{1,0:T(8,128)(2,1)} %all-gather.2.cloned.1.call-done) | copy-start | bytes 28311556
  121.2 1.8 copy-start.6
  127.8 1.1 copy-start.8
  144.8 8.2 %copy-start.7 = (f32[768,1024]{1,0:T(8,128)S(1)}, f32[768,1024]{1,0:T(8,128)}, u32[]{:S(2)}) copy-start(f32[768,1024]{1,0:T(8,128)} %copy-done.6) | copy-start | bytes 9437188
  144.8 129.4 %reduce-scatter.7.cloned.1.call-start = ((), (), s32[]{:S(2)}) async-start(), calls=%async_computation.5 | async-start | bytes 8912896
  180.9 1.1 copy-start.1
  180.9 1.2 copy-start.2
Sparse Core Ops, SparseCore 0:
  10.2 60.4 all-gather.1
  144.9 40.1 reduce-scatter.4
  188.5 85.6 reduce-scatter.6
